TPU v7x, 32 devices: a whole 2x2x4 slice. The times are simulated.
32 devices in a mesh: rep: 2 (over x), fs: 8 (over z, y), tp: 2 (over core).
Axes of the slice: x: 2, y: 2, z: 4, core: 2. Of those that a mesh axis runs over, the one named last changes fastest.
Arguments:
- tokens: bfloat16 [16, 64, 2048], P(('rep', 'fs'), None, 'tp'), may hold values from -6 to 6
- lin_weight: bfloat16 [2048, 1024], P('fs', 'tp'), may hold values from -0.125 to 0.125
- glu_weight: bfloat16 [2048, 1024], P('fs', 'tp'), may hold values from -0.125 to 0.125
- conv_taps: float32 [31, 1024], P(None, 'tp'), may hold values from -4 to 4
- conv_gain: float32 [1024], P('tp'), may hold values from 0.1 to 1.9
- conv_out_weight: bfloat16 [1024, 2048], P('tp', 'fs'), may hold values from -0.1875 to 0.1875
- mix_gain: float32 [2048], replicated, may hold values from 0.1 to 1.9
- ff_gate: bfloat16 [2048, 5632], P('fs', 'tp'), may hold values from -0.125 to 0.125
- ff_up: bfloat16 [2048, 5632], P('fs', 'tp'), may hold values from -0.125 to 0.125
- ff_down: bfloat16 [5632, 2048], P('tp', 'fs'), may hold values from -0.078125 to 0.078125
- out_gain: float32 [2048], replicated, may hold values from 0.1 to 1.9
Outputs:
- encoded: bfloat16 [16, 64, 2048], P(('rep', 'fs'), None, 'tp')
All inputs are finite; a program needn't handle non-finite values.
Results may differ from a plain program's by a relative error of at most 0.014.
Values may be sent and summed in bfloat16 or wider, within the bound.
A program may use at most 128 MiB of HBM per device.

v0:
```python
import jax
import jax.numpy as jnp
from jax import lax
from jax.sharding import PartitionSpec as P

residual_scale = 2.0**0.25
epsilon = 1e-05


def normed(values):
    average = jnp.mean(values, axis=-1, keepdims=True)
    second = jnp.mean(values * values, axis=-1, keepdims=True)
    return (values - average) * lax.rsqrt(second - average * average + epsilon)


def interleave(left, right, parts):
    rows, width = left.shape
    pair = jnp.concatenate(
        (left.reshape(rows, parts, width // parts), right.reshape(rows, parts, width // parts)),
        axis=2,
    )
    return pair.reshape(rows, 2 * width)


def on_device(
    tokens,
    lin_weight,
    glu_weight,
    conv_taps,
    conv_gain_all,
    conv_out_weight,
    mix_gain,
    ff_gate,
    ff_up,
    ff_down,
    out_gain,
):
    n_fs, n_tp = (lax.axis_size("fs"), lax.axis_size("tp"))
    fs_index, tp_index = (lax.axis_index("fs"), lax.axis_index("tp"))
    seqs, length, feat = tokens.shape
    groups = n_fs * seqs
    rows = groups * length
    model = feat * n_tp
    gathered = lax.all_gather(tokens, ("fs", "tp"), axis=0, tiled=False)
    all_tokens = (
        gathered.reshape(n_fs, n_tp, seqs, length, feat)
        .transpose(0, 2, 3, 1, 4)
        .reshape(rows, model)
    )
    glu_pair = lax.all_to_all(
        interleave(lin_weight, glu_weight, n_fs), "fs", split_axis=1, concat_axis=0, tiled=True
    )
    own_out = lax.all_to_all(conv_out_weight, "tp", split_axis=1, concat_axis=0, tiled=True)
    ff_pair = lax.all_to_all(
        interleave(ff_gate, ff_up, n_fs), "fs", split_axis=1, concat_axis=0, tiled=True
    )
    own_down = lax.all_to_all(ff_down, "fs", split_axis=0, concat_axis=1, tiled=True)
    chans = glu_pair.shape[1] // 2
    product = jnp.dot(all_tokens, glu_pair, preferred_element_type=jnp.float32)
    glu = (product[:, :chans] * jax.nn.sigmoid(product[:, chans:])).astype(jnp.bfloat16)
    n_taps = conv_taps.shape[0]
    margin = (n_taps - 1) // 2
    own_taps = lax.dynamic_slice_in_dim(conv_taps, fs_index * chans, chans, 1)
    padded = jnp.pad(
        glu.astype(jnp.float32).reshape(groups, length, chans), ((0, 0), (margin, margin), (0, 0))
    )
    conv = sum((padded[:, k : k + length] * own_taps[k] for k in range(n_taps)))
    conv = conv.reshape(rows, chans).astype(jnp.bfloat16)
    conv_all = lax.all_gather(conv, ("tp", "fs"), axis=1, tiled=True)
    activated = jax.nn.silu(normed(conv_all.astype(jnp.float32)) * conv_gain_all).astype(
        jnp.bfloat16
    )
    mixed_own = jnp.dot(activated, own_out, preferred_element_type=jnp.float32).astype(jnp.bfloat16)
    mixed = lax.all_gather(mixed_own, ("fs", "tp"), axis=1, tiled=True)
    before = residual_scale * all_tokens.astype(jnp.float32) + mixed.astype(jnp.float32)
    middle = (normed(before) * mix_gain).astype(jnp.bfloat16)
    units = ff_pair.shape[1] // 2
    both = jnp.dot(middle, ff_pair, preferred_element_type=jnp.float32)
    hidden = (jax.nn.silu(both[:, :units]) * both[:, units:]).astype(jnp.bfloat16)
    down = jnp.dot(hidden, own_down, preferred_element_type=jnp.float32).astype(jnp.bfloat16)
    sends = (
        down.reshape(n_fs, seqs * length, n_tp, feat)
        .transpose(0, 2, 1, 3)
        .reshape(n_fs * n_tp, seqs * length, feat)
    )
    arrived = lax.all_to_all(sends, ("fs", "tp"), split_axis=0, concat_axis=0, tiled=True)
    forward = jnp.sum(arrived.astype(jnp.float32), axis=0)
    forward = forward.astype(jnp.bfloat16).astype(jnp.float32)
    middle_own = lax.dynamic_slice(
        middle, (fs_index * seqs * length, tp_index * feat), (seqs * length, feat)
    )
    final = residual_scale * middle_own.astype(jnp.float32) + forward
    sums, squares = lax.psum(
        (jnp.sum(final, axis=1, keepdims=True), jnp.sum(final * final, axis=1, keepdims=True)), "tp"
    )
    average = sums / model
    out = (final - average) * lax.rsqrt(squares / model - average * average + epsilon)
    gain = lax.dynamic_slice_in_dim(out_gain, tp_index * feat, feat, 0)
    return (out * gain).astype(jnp.bfloat16).reshape(seqs, length, feat)


def solution(mesh):
    mapped = jax.shard_map(
        on_device,
        mesh=mesh,
        in_specs=(
            P(("rep", "fs"), None, "tp"),
            P("fs", "tp"),
            P("fs", "tp"),
            P(None, "tp"),
            P(),
            P("tp", "fs"),
            P(),
            P("fs", "tp"),
            P("fs", "tp"),
            P("tp", "fs"),
            P(),
        ),
        out_specs=P(("rep", "fs"), None, "tp"),
        check_vma=False,
    )
    return mapped
```

profile of v0, /device:TPU:17, one launch (start us, length us, event | category | flops | bytes accessed | tf_op | source)
XLA Modules:
  0.0 278.2 jit_solution(18404688022100981771)
XLA Ops:
  6.5 0.0 all-gather.11.cloned.1.call-start
  6.5 0.7 all-gather.11.cloned.1.call-update
  7.3 1.1 copy.34
  8.3 1.1 copy.35
  9.4 0.8 pad_maximum_fusion.1
  10.3 5.6 %all-to-all-start = ((bf16[256,8,128]{0,2,1:T(8,128)(2,1)}), bf16[256,8,128]{0,2,1:T(8,128)(2,1)S(1)}, u32[]{:S(2)}, u32[]{:S(2)}) async-start(bf16[256,8,128]{0,2,1:T(8,128)(2,1)} %pad_maximum_fusion.1), calls=%async_computation | async-start | bytes 1048576 | tf_op jit(solution)/shard_map/all_to_all | solution.py:50
  15.9 0.0 copy-done.5
  15.9 0.8 copy.37
  16.7 1.6 dynamic-slice_bitcast_fusion.29
  18.4 1.8 dynamic-slice_bitcast_fusion.30
  20.2 11.9 %all-to-all-done = bf16[256,8,128]{0,2,1:T(8,128)(2,1)S(1)} async-done(((bf16[256,8,128]{0,2,1:T(8,128)(2,1)}), bf16[256,8,128]{0,2,1:T(8,128)(2,1)S(1)}, u32[]{:S(2)}, u32[]{:S(2)}) %all-to-all-start) | async-done | bytes 524320 | tf_op jit(solution)/shard_map/all_to_all | solution.py:50
  32.0 4.2 %all-to-all-start.1 = ((bf16[512,2,128]{0,2,1:T(8,128)(2,1)}), bf16[512,2,128]{0,2,1:T(8,128)(2,1)S(1)}, u32[]{:S(2)}, u32[]{:S(2)}) async-start(bf16[512,2,128]{0,2,1:T(8,128)(2,1)} %bitcast.40), calls=%async_computation.1 | async-start | bytes 524288 | tf_op jit(solution)/shard_map/all_to_all | solution.py:53
  36.2 1.0 copy.36
  37.2 16.4 %all-gather.11.cloned.1.call-done = bf16[16,64,1024]{2,1,0:T(8,128)(2,1)} async-done(((bf16[1,64,1024]{2,1,0:T(8,128)(2,1)}), bf16[16,64,1024]{2,1,0:T(8,128)(2,1)}) %all-gather.11.cloned.1.call-update) | async-done | bytes 2097168 | tf_op jit(solution)/shard_map/all_gather | solution.py:44
  53.7 3.7 %copy.33 = bf16[8,2,1,64,1024]{4,1,3,0,2:T(2,128)(2,1)S(1)} copy(bf16[8,2,1,64,1024]{4,3,1,0,2:T(8,128)(2,1)} %bitcast.118) | data formatting | bytes 4194304 | tf_op jit(solution)/shard_map/reshape | solution.py:46
  57.4 0.6 copy.46
  58.0 0.0 all-to-all-done.1
  58.0 0.0 copy-start.4
  58.0 0.7 copy-done.4
  58.8 5.5 %all-to-all-start.3 = ((bf16[8,352,256]{2,1,0:T(8,128)(2,1)}), bf16[8,352,256]{2,1,0:T(8,128)(2,1)S(1)}, u32[]{:S(2)}, u32[]{:S(2)}) async-start(bf16[8,352,256]{2,1,0:T(8,128)(2,1)} %bitcast.121), calls=%async_computation.3 | async-start | bytes 2883584 | tf_op jit(solution)/shard_map/all_to_all | solution.py:57
  64.3 0.0 all-gather.7.cloned.1.call-start
  64.3 1.9 convolution_bitcast_fusion
  66.1 0.7 fusion.36
  66.8 1.7 reshape.133
  68.6 12.1 %add_convert_fusion = bf16[8,64,64]{1,0,2:T(8,128)(2,1)} fusion(f32[8,64,64]{1,0,2:T(8,128)} %reshape.133, f32[64]{0:T(128)} %get-tuple-element.43, f32[64]{0:T(128)S(1)} %get-tuple-element.14, f32[64]{0:T(128)S(1)} %get-tuple-element.15, f32[64]{0:T(128)S(1)} %get-tuple-element.16, f32[64]{0:T(128)} %get-tuple-element.17, f32[64]{0:T(128)} %get-tuple-element.18, ...), kind=kLoop, calls=%fused_computation.27 | loop fusion | flops 2031616 | bytes 204544 | tf_op jit(solution)/shard_map/convert_element_type | solution.py:68
  80.6 1.7 convert_element_type.50
  82.3 0.0 all-gather.7.cloned.1.call-update
  82.4 2.6 copy.39
  84.9 2.5 copy.40
  87.5 3.6 %pad_maximum_fusion = bf16[256,8,704]{0,2,1:T(8,128)(2,1)} fusion(bf16[256,8,352]{0,2,1:T(8,128)(2,1)} %bitcast.116, bf16[256,8,352]{0,2,1:T(8,128)(2,1)} %bitcast.115), kind=kLoop, calls=%fused_computation.8 | loop fusion | flops 5767168 | bytes 5767168 | tf_op jit(solution)/shard_map/concatenate | solution.py:18
  91.0 5.2 %all-to-all-done.3 = bf16[8,352,256]{2,1,0:T(8,128)(2,1)S(1)} async-done(((bf16[8,352,256]{2,1,0:T(8,128)(2,1)}), bf16[8,352,256]{2,1,0:T(8,128)(2,1)S(1)}, u32[]{:S(2)}, u32[]{:S(2)}) %all-to-all-start.3) | async-done | bytes 1441824 | tf_op jit(solution)/shard_map/all_to_all | solution.py:57
  96.2 7.6 %all-to-all-start.2 = ((bf16[256,8,704]{0,2,1:T(8,128)(2,1)}), bf16[256,8,704]{0,2,1:T(8,128)(2,1)}, u32[]{:S(2)}, u32[]{:S(2)}) async-start(bf16[256,8,704]{0,2,1:T(8,128)(2,1)} %pad_maximum_fusion), calls=%async_computation.2 | async-start | bytes 5767168 | tf_op jit(solution)/shard_map/all_to_all | solution.py:54
  103.8 0.0 all-gather.9.cloned.1.call-start
  103.8 1.8 copy.38
  105.6 0.0 copy-done.7
  105.6 3.2 %all-gather.2 = f32[2,1,512]{2,1,0:T(1,128)S(1)} all-gather(f32[1,1,512]{2,1,0:T(1,128)S(1)} %bitcast.128), channel_id=3, replica_groups=mesh['rep'=2,'fs'=8,'tp'=2] {'tp'}, dimensions={0}, use_global_device_ids=true | all-gather | bytes 6144 | tf_op args[4]
  108.8 19.7 %all-gather.7.cloned.1.call-done = bf16[512,1024]{0,1:T(8,128)(2,1)} async-done(((bf16[512,64]{0,1:T(8,128)(2,1)}), bf16[512,1024]{0,1:T(8,128)(2,1)}) %all-gather.7.cloned.1.call-update) | async-done | bytes 1048592 | tf_op jit(solution)/shard_map/all_gather | solution.py:69
  128.5 1.6 convert_reduce_fusion
  130.0 2.9 %convolution_convert_fusion.1 = bf16[512,128]{1,0:T(8,128)(2,1)} fusion(bf16[1024,128]{1,0:T(8,128)(2,1)} %bitcast.126, bf16[512,1024]{0,1:T(8,128)(2,1)} %all-gather.7.cloned.1.call-done, f32[1024]{0:T(1024)S(1)} %bitcast.127, f32[512]{0:T(512)S(1)} %get-tuple-element.47, f32[512]{0:T(512)S(1)} %get-tuple-element.46), kind=kOutput, calls=%fused_computation.19 | convolution fusion | flops 139001856 | bytes 1449984 | tf_op jit(solution)/shard_map/dot_general | solution.py:73
  133.0 0.0 all-gather.9.cloned.1.call-update
  133.0 1.4 copy.45
  134.4 38.2 %all-to-all-done.2 = bf16[256,8,704]{0,2,1:T(8,128)(2,1)} async-done(((bf16[256,8,704]{0,2,1:T(8,128)(2,1)}), bf16[256,8,704]{0,2,1:T(8,128)(2,1)}, u32[]{:S(2)}, u32[]{:S(2)}) %all-to-all-start.2) | async-done | bytes 2883616 | tf_op jit(solution)/shard_map/all_to_all | solution.py:54
  172.6 3.8 %copy.44 = bf16[8,88,8,256]{3,2,0,1:T(8,128)(2,1)} copy(bf16[8,88,8,256]{3,2,1,0:T(8,128)(2,1)} %bitcast.56) | data formatting | bytes 5767168 | tf_op jit(solution)/shard_map/all_to_all | solution.py:54
  176.4 22.5 %all-gather.9.cloned.1.call-done = bf16[512,2048]{1,0:T(8,128)(2,1)} async-done(((bf16[512,128]{1,0:T(8,128)(2,1)}), bf16[512,2048]{1,0:T(8,128)(2,1)}) %all-gather.9.cloned.1.call-update) | async-done | bytes 2097168 | tf_op jit(solution)/shard_map/all_gather | solution.py:74
  198.9 2.8 %fusion = (f32[512]{0:T(512)S(1)}, f32[512]{0:T(512)S(1)}) fusion(bf16[512,2048]{1,0:T(8,128)(2,1)} %all-gather.9.cloned.1.call-done, bf16[512,2048]{1,0:T(8,128)(2,1)S(1)} %bitcast.110), kind=kLoop, calls=%fused_computation.3 | loop fusion | flops 7339008 | bytes 4198400 | tf_op jit(solution)/shard_map/reduce_sum | solution.py:11
  201.7 0.0 copy-done.6
  201.7 0.0 copy-done
  201.7 0.0 copy-start.1
  201.7 1.1 multiply_convert_fusion
  202.8 0.0 copy-start.2
  202.8 0.7 copy-done.1
  203.5 1.7 fusion.39
  205.2 0.0 copy-done.2
  205.2 0.0 copy-done.3
  205.2 2.7 convolution_convert_fusion
  207.9 3.3 %reshape.129 = bf16[8,64,2,1024]{3,2,1,0:T(2,128)(2,1)S(1)} reshape(bf16[512,2048]{1,0:T(8,128)(2,1)} %convolution_convert_fusion) | data formatting | bytes 4194304 | tf_op jit(solution)/shard_map/reshape | solution.py:82
  211.2 2.0 copy.43
  213.2 5.2 %all-to-all-start.4 = ((bf16[16,64,1024]{2,1,0:T(8,128)(2,1)}), bf16[16,64,1024]{2,1,0:T(8,128)(2,1)S(1)}, u32[]{:S(2)}, u32[]{:S(2)}) async-start(bf16[16,64,1024]{2,1,0:T(8,128)(2,1)} %bitcast.112), calls=%async_computation.4 | async-start | bytes 4194304 | tf_op jit(solution)/shard_map/all_to_all | solution.py:86
  218.4 47.0 %all-to-all-done.4 = bf16[16,64,1024]{2,1,0:T(8,128)(2,1)S(1)} async-done(((bf16[16,64,1024]{2,1,0:T(8,128)(2,1)}), bf16[16,64,1024]{2,1,0:T(8,128)(2,1)S(1)}, u32[]{:S(2)}, u32[]{:S(2)}) %all-to-all-start.4) | async-done | bytes 2097184 | tf_op jit(solution)/shard_map/all_to_all | solution.py:86
  265.5 0.4 reduce_sum.70
  265.9 1.1 fusion.29
  266.9 3.1 %all-reduce.1 = (f32[64,1]{0,1:T(1,128)S(1)}, f32[64,1]{0,1:T(1,128)S(1)}) all-reduce(f32[64,1]{0,1:T(1,128)S(1)} %bitcast.130, f32[64,1]{0,1:T(1,128)S(1)} %bitcast.129), channel_id=1, replica_groups=mesh['rep'=2,'fs'=8,'tp'=2] {'tp'}, use_global_device_ids=true, to_apply=%region_8.9 | all-reduce | flops 128 | bytes 1024 | tf_op jit(solution)/shard_map/psum | solution.py:93
  270.0 0.0 dynamic-slice-done
  270.0 1.7 fusion.30
  (9 shorter events, 0.0 us)
Async XLA Ops:
  6.5 9.3 %copy-start.5 = (bf16[512,256]{1,0:T(8,128)(2,1)S(1)}, bf16[512,256]{1,0:T(8,128)(2,1)}, u32[]{:S(2)}) copy-start(bf16[512,256]{1,0:T(8,128)(2,1)} %param.16) | copy-start | bytes 786436
  6.5 47.1 %all-gather.11.cloned.1.call-start = ((), (), s32[]{:S(2)}) async-start(), calls=%async_computation.7 | async-start | bytes 2228224 | tf_op jit(solution)/shard_map/all_gather | solution.py:44
  10.3 21.7 %all-to-all-start = ((bf16[256,8,128]{0,2,1:T(8,128)(2,1)}), bf16[256,8,128]{0,2,1:T(8,128)(2,1)S(1)}, u32[]{:S(2)}, u32[]{:S(2)}) async-start(bf16[256,8,128]{0,2,1:T(8,128)(2,1)} %pad_maximum_fusion.1), calls=%async_computation | async-start | bytes 1048576 | tf_op jit(solution)/shard_map/all_to_all | solution.py:50
  32.0 26.0 %all-to-all-start.1 = ((bf16[512,2,128]{0,2,1:T(8,128)(2,1)}), bf16[512,2,128]{0,2,1:T(8,128)(2,1)S(1)}, u32[]{:S(2)}, u32[]{:S(2)}) async-start(bf16[512,2,128]{0,2,1:T(8,128)(2,1)} %bitcast.40), calls=%async_computation.1 | async-start | bytes 524288 | tf_op jit(solution)/shard_map/all_to_all | solution.py:53
  58.0 0.7 copy-start.4
  58.8 37.5 %all-to-all-start.3 = ((bf16[8,352,256]{2,1,0:T(8,128)(2,1)}), bf16[8,352,256]{2,1,0:T(8,128)(2,1)S(1)}, u32[]{:S(2)}, u32[]{:S(2)}) async-start(bf16[8,352,256]{2,1,0:T(8,128)(2,1)} %bitcast.121), calls=%async_computation.3 | async-start | bytes 2883584 | tf_op jit(solution)/shard_map/all_to_all | solution.py:57
  64.3 64.2 %all-gather.7.cloned.1.call-start = ((), (), s32[]{:S(2)}) async-start(), calls=%async_computation.5 | async-start | bytes 1114112 | tf_op jit(solution)/shard_map/all_gather | solution.py:69
  91.0 14.6 %copy-start.7 = (f32[512]{0:T(512)S(1)}, f32[512]{0:T(512)}, u32[]{:S(2)}) copy-start(f32[512]{0:T(512)} %param.15) | copy-start | bytes 6148
  96.2 76.3 %all-to-all-start.2 = ((bf16[256,8,704]{0,2,1:T(8,128)(2,1)}), bf16[256,8,704]{0,2,1:T(8,128)(2,1)}, u32[]{:S(2)}, u32[]{:S(2)}) async-start(bf16[256,8,704]{0,2,1:T(8,128)(2,1)} %pad_maximum_fusion), calls=%async_computation.2 | async-start | bytes 5767168 | tf_op jit(solution)/shard_map/all_to_all | solution.py:54
  103.8 95.1 %all-gather.9.cloned.1.call-start = ((), (), s32[]{:S(2)}) async-start(), calls=%async_computation.6 | async-start | bytes 2228224 | tf_op jit(solution)/shard_map/all_gather | solution.py:74
  176.4 25.3 %copy-start.6 = (f32[2048]{0:T(1024)S(1)}, f32[2048]{0:T(1024)}, u32[]{:S(2)}) copy-start(f32[2048]{0:T(1024)} %param.17) | copy-start | bytes 24580
  198.9 2.8 %copy-start = (bf16[512,2048]{1,0:T(8,128)(2,1)S(1)}, bf16[512,2048]{1,0:T(8,128)(2,1)}, u32[]{:S(2)}) copy-start(bf16[512,2048]{1,0:T(8,128)(2,1)} %all-gather.9.cloned.1.call-done) | copy-start | bytes 6291460
  201.7 1.8 copy-start.1
  202.8 2.4 copy-start.2
  203.5 1.7 copy-start.3
  213.2 52.3 %all-to-all-start.4 = ((bf16[16,64,1024]{2,1,0:T(8,128)(2,1)}), bf16[16,64,1024]{2,1,0:T(8,128)(2,1)S(1)}, u32[]{:S(2)}, u32[]{:S(2)}) async-start(bf16[16,64,1024]{2,1,0:T(8,128)(2,1)} %bitcast.112), calls=%async_computation.4 | async-start | bytes 4194304 | tf_op jit(solution)/shard_map/all_to_all | solution.py:86
  218.4 51.6 %dynamic-slice-start = ((f32[2048]{0:T(1024)}, s32[]{:T(128)}), f32[1024]{0:T(1024)S(1)}, s32[]{:S(2)}) async-start(f32[2048]{0:T(1024)} %param.21, s32[]{:T(128)} %select_n.9), calls=%async_computation.8 | async-start | bytes 8704 | tf_op jit(solution)/shard_map/dynamic_slice | solution.py:98
Sparse Core Ops, SparseCore 0:
  9.5 44.1 all-gather.10
  82.5 45.9 all-gather.6
  133.1 65.7 all-gather.8
where the time goes:
time: 279 us; the launch traced here: 278 us
  waiting for transfers between devices  162 us (58%)
  local copies, waits for them, and re-layouts  34 us (12%)
  starting transfers between devices  28.1 us (10%)
  other arithmetic  25.8 us (9%)
  between operations  13.3 us (5%)
  matrix products  9.17 us (3%)
  blocking collectives  6.25 us (2%)
    all_to_all x1, waiting for transfers between devices, on_device(): lax.all_to_all(sends, ('fs', 'tp'), split_axis=0, concat_axis=0, tiled=True)  47 us
    all_to_all x1, waiting for transfers between devices, on_device(): lax.all_to_all(interleave(ff_gate, ff_up, n_fs), 'fs', split_axis=1, conc...  38.2 us
    all_gather x1, waiting for transfers between devices, on_device(): mixed = lax.all_gather(mixed_own, ('fs', 'tp'), axis=1, tiled=True)  22.5 us
    all_gather x1, waiting for transfers between devices, on_device(): conv_all = lax.all_gather(conv, ('tp', 'fs'), axis=1, tiled=True)  19.7 us
    all_gather x1, waiting for transfers between devices, on_device(): gathered = lax.all_gather(tokens, ('fs', 'tp'), axis=0, tiled=False)  16.4 us
    convert_element_type x1, other arithmetic, on_device(): conv = conv.reshape(rows, chans).astype(jnp.bfloat16)  12.1 us
    all_to_all x1, waiting for transfers between devices, on_device(): lax.all_to_all(interleave(lin_weight, glu_weight, n_fs), 'fs', split_axis...  11.9 us
    unnamed x22, local copies, waits for them, and re-layouts  10.2 us
  transfers between devices with their start and end apart: 8, of which 7 were waited for; matrix products, arithmetic and copies ran while one was open for 18% of the time, Pallas kernels for 0%

commit v1 on v0

--- a/solution.py
+++ b/solution.py
@@ -51,8 +51,14 @@
         interleave(lin_weight, glu_weight, n_fs), "fs", split_axis=1, concat_axis=0, tiled=True
     )
     own_out = lax.all_to_all(conv_out_weight, "tp", split_axis=1, concat_axis=0, tiled=True)
-    ff_pair = lax.all_to_all(
-        interleave(ff_gate, ff_up, n_fs), "fs", split_axis=1, concat_axis=0, tiled=True
+    ff_pair = jnp.concatenate(
+        lax.all_to_all(
+            jnp.stack(jnp.split(interleave(ff_gate, ff_up, n_fs), lax.axis_size("fs"), axis=1)),
+            "fs",
+            0,
+            0,
+        ),
+        axis=0,
     )
     own_down = lax.all_to_all(ff_down, "fs", split_axis=0, concat_axis=1, tiled=True)
     chans = glu_pair.shape[1] // 2

time: 279 us -> 280 us (level)
  local copies, waits for them, and re-layouts: 34 us -> 41.5 us
  waiting for transfers between devices: 162 us -> 156 us
    unnamed x22 -> x35, local copies, waits for them, and re-layouts: 10.2 us -> 16.9 us
    all_to_all x1, waiting for transfers between devices: 11.9 us -> 7.63 us  [on_device(): lax.all_to_all(interleave(lin_weight, glu_weight, n_fs), 'fs', split_axis...]
    all_to_all x1 -> x0, local copies, waits for them, and re-layouts: 3.8 us -> none  [on_device(): lax.all_to_all(interleave(ff_gate, ff_up, n_fs), 'fs', split_axis=1, conc...]
    reshape x0 -> x1, local copies, waits for them, and re-layouts: none -> 3.8 us  [on_device(): jnp.concatenate(lax.all_to_all(jnp.stack(jnp.split(interleave(ff_gate, ff...]
  transfers between devices with their start and end apart: 8 -> 8, of which waited for: 7 -> 7; matrix products, arithmetic and copies ran while one was open for 18% -> 20% of each run, Pallas kernels for 0% -> 0%
where the time goes in v1:
time: 280 us; the launch traced here: 279 us
  waiting for transfers between devices  156 us (56%)
  local copies, waits for them, and re-layouts  41.5 us (15%)
  starting transfers between devices  28.5 us (10%)
  other arithmetic  23.8 us (8%)
  between operations  13.3 us (5%)
  matrix products  9.15 us (3%)
  blocking collectives  6.17 us (2%)
    all_to_all x1, waiting for transfers between devices, on_device(): lax.all_to_all(sends, ('fs', 'tp'), split_axis=0, concat_axis=0, tiled=True)  47 us
    all_to_all x1, waiting for transfers between devices, on_device(): lax.all_to_all(jnp.stack(jnp.split(interleave(ff_gate, ff_up, n_fs), lax....  38.1 us
    all_gather x1, waiting for transfers between devices, on_device(): mixed = lax.all_gather(mixed_own, ('fs', 'tp'), axis=1, tiled=True)  22.4 us
    all_gather x1, waiting for transfers between devices, on_device(): conv_all = lax.all_gather(conv, ('tp', 'fs'), axis=1, tiled=True)  20 us
    unnamed x35, local copies, waits for them, and re-layouts  16.9 us
    all_gather x1, waiting for transfers between devices, on_device(): gathered = lax.all_gather(tokens, ('fs', 'tp'), axis=0, tiled=False)  16.5 us
    convert_element_type x1, other arithmetic, on_device(): conv = conv.reshape(rows, chans).astype(jnp.bfloat16)  11.9 us
    all_to_all x1, starting transfers between devices, on_device(): lax.all_to_all(jnp.stack(jnp.split(interleave(ff_gate, ff_up, n_fs), lax....  7.79 us
  transfers between devices with their start and end apart: 8, of which 7 were waited for; matrix products, arithmetic and copies ran while one was open for 20% of the time, Pallas kernels for 0%

profile of v1, /device:TPU:17, one launch (start us, length us, event | category | flops | bytes accessed | tf_op | source)
XLA Modules:
  0.0 278.5 jit_solution(3357184700737185288)
XLA Ops:
  6.5 0.0 all-gather.11.cloned.1.call-start
  6.5 0.7 all-gather.11.cloned.1.call-update
  7.3 1.1 copy.33
  8.3 1.1 copy.34
  9.4 0.8 pad_maximum_fusion.1
  10.3 5.6 %all-to-all-start = ((bf16[256,8,128]{0,2,1:T(8,128)(2,1)}), bf16[256,8,128]{0,2,1:T(8,128)(2,1)S(1)}, u32[]{:S(2)}, u32[]{:S(2)}) async-start(bf16[256,8,128]{0,2,1:T(8,128)(2,1)} %pad_maximum_fusion.1), calls=%async_computation | async-start | bytes 1048576 | tf_op jit(solution)/shard_map/all_to_all | solution.py:50
  15.9 0.0 copy-done.7
  15.9 0.8 copy.36
  16.7 0.7 copy.38
  17.4 1.7 copy.39
  19.2 1.7 dynamic-slice_bitcast_fusion.29
  20.8 1.8 dynamic-slice_bitcast_fusion.30
  22.6 1.8 pad_maximum_fusion
  24.4 7.6 %all-to-all-done = bf16[256,8,128]{0,2,1:T(8,128)(2,1)S(1)} async-done(((bf16[256,8,128]{0,2,1:T(8,128)(2,1)}), bf16[256,8,128]{0,2,1:T(8,128)(2,1)S(1)}, u32[]{:S(2)}, u32[]{:S(2)}) %all-to-all-start) | async-done | bytes 524320 | tf_op jit(solution)/shard_map/all_to_all | solution.py:50
  32.0 4.2 %all-to-all-start.1 = ((bf16[512,2,128]{0,2,1:T(8,128)(2,1)}), bf16[512,2,128]{0,2,1:T(8,128)(2,1)S(1)}, u32[]{:S(2)}, u32[]{:S(2)}) async-start(bf16[512,2,128]{0,2,1:T(8,128)(2,1)} %bitcast.164), calls=%async_computation.1 | async-start | bytes 524288 | tf_op jit(solution)/shard_map/all_to_all | solution.py:53
  36.2 1.0 copy.35
  37.3 16.5 %all-gather.11.cloned.1.call-done = bf16[16,64,1024]{2,1,0:T(8,128)(2,1)} async-done(((bf16[1,64,1024]{2,1,0:T(8,128)(2,1)}), bf16[16,64,1024]{2,1,0:T(8,128)(2,1)}) %all-gather.11.cloned.1.call-update) | async-done | bytes 2097168 | tf_op jit(solution)/shard_map/all_gather | solution.py:44
  53.8 3.7 %copy.32 = bf16[8,2,1,64,1024]{4,1,3,0,2:T(2,128)(2,1)S(1)} copy(bf16[8,2,1,64,1024]{4,3,1,0,2:T(8,128)(2,1)} %bitcast.158) | data formatting | bytes 4194304 | tf_op jit(solution)/shard_map/reshape | solution.py:46
  57.5 0.6 copy.45
  58.1 0.0 all-to-all-done.1
  58.1 0.0 copy-start.6
  58.1 0.7 copy-done.6
  58.9 5.5 %all-to-all-start.3 = ((bf16[8,352,256]{2,1,0:T(8,128)(2,1)}), bf16[8,352,256]{2,1,0:T(8,128)(2,1)S(1)}, u32[]{:S(2)}, u32[]{:S(2)}) async-start(bf16[8,352,256]{2,1,0:T(8,128)(2,1)} %bitcast.161), calls=%async_computation.3 | async-start | bytes 2883584 | tf_op jit(solution)/shard_map/all_to_all | solution.py:63
  64.4 1.9 convolution_bitcast_fusion
  66.3 0.7 fusion.44
  67.0 1.7 reshape.136
  68.7 11.9 %add_convert_fusion = bf16[8,64,64]{1,0,2:T(8,128)(2,1)} fusion(f32[8,64,64]{1,0,2:T(8,128)} %reshape.136, f32[64]{0:T(128)} %get-tuple-element.43, f32[64]{0:T(128)S(1)} %get-tuple-element.14, f32[64]{0:T(128)S(1)} %get-tuple-element.15, f32[64]{0:T(128)S(1)} %get-tuple-element.16, f32[64]{0:T(128)} %get-tuple-element.17, f32[64]{0:T(128)} %get-tuple-element.18, ...), kind=kLoop, calls=%fused_computation.43 | loop fusion | flops 2031616 | bytes 204544 | tf_op jit(solution)/shard_map/convert_element_type | solution.py:74
  80.6 1.7 convert_element_type.50
  82.3 0.0 all-gather.7.cloned.1.call-update
  82.3 1.9 fusion.20
  84.2 1.8 fusion.19
  86.0 1.8 fusion.18
  87.7 1.7 fusion.17
  89.5 0.0 copy-done
  89.5 0.8 fusion.16
  90.2 0.8 fusion.15
  91.0 0.8 fusion.14
  91.8 0.8 fusion.13
  92.5 3.6 %all-to-all-done.3 = bf16[8,352,256]{2,1,0:T(8,128)(2,1)S(1)} async-done(((bf16[8,352,256]{2,1,0:T(8,128)(2,1)}), bf16[8,352,256]{2,1,0:T(8,128)(2,1)S(1)}, u32[]{:S(2)}, u32[]{:S(2)}) %all-to-all-start.3) | async-done | bytes 1441824 | tf_op jit(solution)/shard_map/all_to_all | solution.py:63
  96.2 7.8 %all-to-all-start.2 = ((bf16[8,256,704]{1,2,0:T(8,128)(2,1)}), bf16[8,256,704]{1,2,0:T(8,128)(2,1)}, u32[]{:S(2)}, u32[]{:S(2)}) async-start(bf16[8,256,704]{1,2,0:T(8,128)(2,1)} %fusion.13), calls=%async_computation.2 | async-start | bytes 5767168 | tf_op jit(solution)/shard_map/all_to_all | solution.py:55
  104.0 1.8 copy.37
  105.8 0.0 copy-done.9
  105.8 3.1 %all-gather.2 = f32[2,1,512]{2,1,0:T(1,128)S(1)} all-gather(f32[1,1,512]{2,1,0:T(1,128)S(1)} %bitcast.169), channel_id=3, replica_groups=mesh['rep'=2,'fs'=8,'tp'=2] {'tp'}, dimensions={0}, use_global_device_ids=true | all-gather | bytes 6144 | tf_op args[4]
  108.8 20.0 %all-gather.7.cloned.1.call-done = bf16[512,1024]{0,1:T(8,128)(2,1)} async-done(((bf16[512,64]{0,1:T(8,128)(2,1)}), bf16[512,1024]{0,1:T(8,128)(2,1)}) %all-gather.7.cloned.1.call-update) | async-done | bytes 1048592 | tf_op jit(solution)/shard_map/all_gather | solution.py:75
  128.9 1.6 convert_reduce_fusion
  130.4 2.9 %convolution_convert_fusion.1 = bf16[512,128]{1,0:T(8,128)(2,1)} fusion(bf16[1024,128]{1,0:T(8,128)(2,1)} %bitcast.167, bf16[512,1024]{0,1:T(8,128)(2,1)} %all-gather.7.cloned.1.call-done, f32[1024]{0:T(1024)S(1)} %bitcast.168, f32[512]{0:T(512)S(1)} %get-tuple-element.47, f32[512]{0:T(512)S(1)} %get-tuple-element.46), kind=kOutput, calls=%fused_computation.19 | convolution fusion | flops 139001856 | bytes 1449984 | tf_op jit(solution)/shard_map/dot_general | solution.py:79
  133.4 0.0 all-gather.9.cloned.1.call-update
  133.4 1.4 copy.44
  134.8 38.1 %all-to-all-done.2 = bf16[8,256,704]{1,2,0:T(8,128)(2,1)} async-done(((bf16[8,256,704]{1,2,0:T(8,128)(2,1)}), bf16[8,256,704]{1,2,0:T(8,128)(2,1)}, u32[]{:S(2)}, u32[]{:S(2)}) %all-to-all-start.2) | async-done | bytes 2883616 | tf_op jit(solution)/shard_map/all_to_all | solution.py:55
  172.8 3.8 %copy.43 = bf16[8,88,8,256]{3,2,0,1:T(8,128)(2,1)} copy(bf16[8,88,8,256]{3,2,1,0:T(8,128)(2,1)} %bitcast.64) | data formatting | bytes 5767168 | tf_op jit(solution)/shard_map/reshape | solution.py:54
  176.7 22.4 %all-gather.9.cloned.1.call-done = bf16[512,2048]{1,0:T(8,128)(2,1)} async-done(((bf16[512,128]{1,0:T(8,128)(2,1)}), bf16[512,2048]{1,0:T(8,128)(2,1)}) %all-gather.9.cloned.1.call-update) | async-done | bytes 2097168 | tf_op jit(solution)/shard_map/all_gather | solution.py:80
  199.1 2.8 %fusion = (f32[512]{0:T(512)S(1)}, f32[512]{0:T(512)S(1)}) fusion(bf16[512,2048]{1,0:T(8,128)(2,1)} %all-gather.9.cloned.1.call-done, bf16[512,2048]{1,0:T(8,128)(2,1)S(1)} %bitcast.142), kind=kLoop, calls=%fused_computation.3 | loop fusion | flops 7339008 | bytes 4198400 | tf_op jit(solution)/shard_map/reduce_sum | solution.py:11
  201.9 1.1 multiply_convert_fusion
  203.0 0.7 copy-done.2
  203.7 1.7 fusion.47
  205.4 2.7 convolution_convert_fusion
  208.1 3.3 %reshape.132 = bf16[8,64,2,1024]{3,2,1,0:T(2,128)(2,1)S(1)} reshape(bf16[512,2048]{1,0:T(8,128)(2,1)} %convolution_convert_fusion) | data formatting | bytes 4194304 | tf_op jit(solution)/shard_map/reshape | solution.py:88
  211.4 2.0 copy.42
  213.3 5.3 %all-to-all-start.4 = ((bf16[16,64,1024]{2,1,0:T(8,128)(2,1)}), bf16[16,64,1024]{2,1,0:T(8,128)(2,1)S(1)}, u32[]{:S(2)}, u32[]{:S(2)}) async-start(bf16[16,64,1024]{2,1,0:T(8,128)(2,1)} %bitcast.152), calls=%async_computation.4 | async-start | bytes 4194304 | tf_op jit(solution)/shard_map/all_to_all | solution.py:92
  218.7 47.0 %all-to-all-done.4 = bf16[16,64,1024]{2,1,0:T(8,128)(2,1)S(1)} async-done(((bf16[16,64,1024]{2,1,0:T(8,128)(2,1)}), bf16[16,64,1024]{2,1,0:T(8,128)(2,1)S(1)}, u32[]{:S(2)}, u32[]{:S(2)}) %all-to-all-start.4) | async-done | bytes 2097184 | tf_op jit(solution)/shard_map/all_to_all | solution.py:92
  265.7 0.4 reduce_sum.70
  266.1 1.1 fusion.37
  267.2 3.1 %all-reduce.1 = (f32[64,1]{0,1:T(1,128)S(1)}, f32[64,1]{0,1:T(1,128)S(1)}) all-reduce(f32[64,1]{0,1:T(1,128)S(1)} %bitcast.171, f32[64,1]{0,1:T(1,128)S(1)} %bitcast.170), channel_id=1, replica_groups=mesh['rep'=2,'fs'=8,'tp'=2] {'tp'}, use_global_device_ids=true, to_apply=%region_8.9 | all-reduce | flops 128 | bytes 1024 | tf_op jit(solution)/shard_map/psum | solution.py:99
  270.3 1.7 fusion.38
  (22 shorter events, 0.1 us)
Async XLA Ops:
  6.5 9.4 %copy-start.7 = (bf16[512,256]{1,0:T(8,128)(2,1)S(1)}, bf16[512,256]{1,0:T(8,128)(2,1)}, u32[]{:S(2)}) copy-start(bf16[512,256]{1,0:T(8,128)(2,1)} %param.16) | copy-start | bytes 786436
  6.5 10.2 %copy-start.4 = (bf16[256,2816]{1,0:T(8,128)(2,1)S(1)}, bf16[256,2816]{1,0:T(8,128)(2,1)}, u32[]{:S(2)}) copy-start(bf16[256,2816]{1,0:T(8,128)(2,1)} %param.18) | copy-start | bytes 4325380
  6.5 47.2 %all-gather.11.cloned.1.call-start = ((), (), s32[]{:S(2)}) async-start(), calls=%async_computation.7 | async-start | bytes 2228224 | tf_op jit(solution)/shard_map/all_gather | solution.py:44
  10.3 21.7 %all-to-all-start = ((bf16[256,8,128]{0,2,1:T(8,128)(2,1)}), bf16[256,8,128]{0,2,1:T(8,128)(2,1)S(1)}, u32[]{:S(2)}, u32[]{:S(2)}) async-start(bf16[256,8,128]{0,2,1:T(8,128)(2,1)} %pad_maximum_fusion.1), calls=%async_computation | async-start | bytes 1048576 | tf_op jit(solution)/shard_map/all_to_all | solution.py:50
  32.0 26.1 %all-to-all-start.1 = ((bf16[512,2,128]{0,2,1:T(8,128)(2,1)}), bf16[512,2,128]{0,2,1:T(8,128)(2,1)S(1)}, u32[]{:S(2)}, u32[]{:S(2)}) async-start(bf16[512,2,128]{0,2,1:T(8,128)(2,1)} %bitcast.164), calls=%async_computation.1 | async-start | bytes 524288 | tf_op jit(solution)/shard_map/all_to_all | solution.py:53
  58.1 0.7 copy-start.6
  58.9 37.3 %all-to-all-start.3 = ((bf16[8,352,256]{2,1,0:T(8,128)(2,1)}), bf16[8,352,256]{2,1,0:T(8,128)(2,1)S(1)}, u32[]{:S(2)}, u32[]{:S(2)}) async-start(bf16[8,352,256]{2,1,0:T(8,128)(2,1)} %bitcast.161), calls=%async_computation.3 | async-start | bytes 2883584 | tf_op jit(solution)/shard_map/all_to_all | solution.py:63
  64.4 64.5 %all-gather.7.cloned.1.call-start = ((), (), s32[]{:S(2)}) async-start(), calls=%async_computation.5 | async-start | bytes 1114112 | tf_op jit(solution)/shard_map/all_gather | solution.py:75
  82.3 7.2 %copy-start = (bf16[256,8,704]{0,2,1:T(8,128)(2,1)S(1)}, bf16[256,8,704]{0,2,1:T(8,128)(2,1)}, u32[]{:S(2)}) copy-start(bf16[256,8,704]{0,2,1:T(8,128)(2,1)} %pad_maximum_fusion) | copy-start | bytes 8650756
  92.5 13.2 %copy-start.9 = (f32[512]{0:T(512)S(1)}, f32[512]{0:T(512)}, u32[]{:S(2)}) copy-start(f32[512]{0:T(512)} %param.15) | copy-start | bytes 6148
  96.2 76.7 %all-to-all-start.2 = ((bf16[8,256,704]{1,2,0:T(8,128)(2,1)}), bf16[8,256,704]{1,2,0:T(8,128)(2,1)}, u32[]{:S(2)}, u32[]{:S(2)}) async-start(bf16[8,256,704]{1,2,0:T(8,128)(2,1)} %fusion.13), calls=%async_computation.2 | async-start | bytes 5767168 | tf_op jit(solution)/shard_map/all_to_all | solution.py:55
  104.0 95.1 %all-gather.9.cloned.1.call-start = ((), (), s32[]{:S(2)}) async-start(), calls=%async_computation.6 | async-start | bytes 2228224 | tf_op jit(solution)/shard_map/all_gather | solution.py:80
  176.7 25.2 %copy-start.8 = (f32[2048]{0:T(1024)S(1)}, f32[2048]{0:T(1024)}, u32[]{:S(2)}) copy-start(f32[2048]{0:T(1024)} %param.17) | copy-start | bytes 24580
  199.1 2.8 %copy-start.1 = (bf16[512,2048]{1,0:T(8,128)(2,1)S(1)}, bf16[512,2048]{1,0:T(8,128)(2,1)}, u32[]{:S(2)}) copy-start(bf16[512,2048]{1,0:T(8,128)(2,1)} %all-gather.9.cloned.1.call-done) | copy-start | bytes 6291460
  201.9 1.8 copy-start.2
  202.9 2.5 copy-start.3
  203.7 1.7 copy-start.5
  213.3 5.3 %copy-start.10 = (f32[2048]{0:T(1024)S(1)}, f32[2048]{0:T(1024)}, u32[]{:S(2)}) copy-start(f32[2048]{0:T(1024)} %param.21) | copy-start | bytes 24580
  213.3 52.4 %all-to-all-start.4 = ((bf16[16,64,1024]{2,1,0:T(8,128)(2,1)}), bf16[16,64,1024]{2,1,0:T(8,128)(2,1)S(1)}, u32[]{:S(2)}, u32[]{:S(2)}) async-start(bf16[16,64,1024]{2,1,0:T(8,128)(2,1)} %bitcast.152), calls=%async_computation.4 | async-start | bytes 4194304 | tf_op jit(solution)/shard_map/all_to_all | solution.py:92
Sparse Core Ops, SparseCore 0:
  9.5 44.2 all-gather.10
  82.4 46.3 all-gather.6
  133.5 65.4 all-gather.8
